TPU v7x, 32 devices: a whole 2x2x4 slice. The times are simulated.
32 devices in a mesh: grp: 2 (over y), sp: 8 (over z, core), tp: 2 (over x).
Axes of the slice: x: 2, y: 2, z: 4, core: 2. Of those that a mesh axis runs over, the one named last changes fastest.
Arguments:
- queries_a: bfloat16 [4096, 2, 512], P(('grp', 'sp'), None, 'tp'), parts along dimension 0, may hold values from -120 to 120
- keys_a: bfloat16 [4096, 2, 512], P(('grp', 'sp'), None, 'tp'), parts along dimension 0, may hold values from -6 to 6
- values_a: bfloat16 [4096, 1024], P(('grp', 'sp'), 'tp'), parts along dimension 0, may hold values from -6 to 6
- queries_b: bfloat16 [4096, 2, 512], P(('grp', 'sp'), None, 'tp'), parts along dimension 0, may hold values from -120 to 120
- keys_b: bfloat16 [4096, 2, 512], P(('grp', 'sp'), None, 'tp'), parts along dimension 0, may hold values from -6 to 6
- values_b: bfloat16 [4096, 1024], P(('grp', 'sp'), 'tp'), parts along dimension 0, may hold values from -6 to 6
- lambdas: float32 [12], replicated, may hold values from 0.3 to 0.8
- head_gain_a: float32 [256], replicated, may hold values from 0.1 to 1.9
- head_gain_b: float32 [128], replicated, may hold values from 0.1 to 1.9
- out_a: bfloat16 [1024, 2048], P('tp'), may hold values from -0.125 to 0.125
- out_b: bfloat16 [1024, 2048], P('tp'), may hold values from -0.125 to 0.125
- residual: bfloat16 [4096, 2048], P(('grp', 'sp', 'tp')), parts along dimension 0, may hold values from -6 to 6
- gain_mix: float32 [2048], replicated, may hold values from 0.1 to 1.9
- gain_pre: float32 [2048], replicated, may hold values from 0.1 to 1.9
- gain_post: float32 [2048], replicated, may hold values from 0.1 to 1.9
- routes: int32 [4096, 4], P(('grp', 'sp', 'tp')), parts along dimension 0, may hold values from 0 to 7, all different within a row; in each aligned block of 128 rows (0 to 127, 128 to 255, ...) at most 80 rows name the same one
- route_weights: float32 [4096, 4], P(('grp', 'sp', 'tp')), parts along dimension 0, may hold values from 0.05 to 1
- expert_gate: bfloat16 [8, 2048, 2048], P('sp', None, 'tp'), may hold values from -1 to 1
- expert_up: bfloat16 [8, 2048, 2048], P('sp', None, 'tp'), may hold values from -1 to 1
- expert_down: bfloat16 [8, 2048, 2048], P('sp', 'tp'), may hold values from -0.125 to 0.125
Outputs:
- layer_out: bfloat16 [4096, 2048], P(('grp', 'sp', 'tp')), parts along dimension 0
There are 2 independent parts, one for each index of `grp`. A program takes and returns all parts, laid end to end along the dimension named above; an argument that names none is the same for every part. Nothing has to cross between parts.
Inputs may be any that keep to these rules, and one draw needn't show every extreme that they name: `routes`: in each aligned block of 128 rows (the rows of one device) no expert is named by more than 80 rows, a bound that some blocks reach.
All inputs are finite; a program needn't handle non-finite values.
Results may differ from a plain program's by a relative error of at most 0.018.
Values may be sent and summed in bfloat16 or wider, within the bound.
A program may use at most 128 MiB of HBM per device.

v0:
```python
import jax
import jax.numpy as jnp
from jax import lax
from jax.sharding import PartitionSpec as P

HA = 4
DA = 128
DB = 64


def rms_norm(values, gain_vec):
    return values * lax.rsqrt(jnp.mean(values * values, -1, keepdims=True) + 1e-06) * gain_vec


def attend(current, query_rows, key_rows, value_rows, first_row, query_pos, head_size):
    run_max, run_sum, run_acc = current
    key_count = key_rows.shape[0]
    heads = query_rows.shape[2]
    key_view = key_rows.reshape(key_count, 2, heads, head_size)
    value_view = value_rows.reshape(key_count, heads, 2 * head_size)
    key_pos = first_row + jnp.arange(key_count, dtype=jnp.int32)
    visible = (key_pos[None, :] <= query_pos[:, None])[None, :, None, :]
    scores = jnp.einsum(
        "qmhd,kmhd->mqhk", query_rows, key_view, preferred_element_type=jnp.float32
    ) * head_size ** (-0.5)
    scores = jnp.where(visible, scores, -1e30)
    new_max = jnp.maximum(run_max, jnp.max(scores, -1))
    exp_terms = jnp.where(visible, jnp.exp(scores - new_max[..., None]), 0.0)
    rescale = jnp.exp(run_max - new_max)
    run_sum = run_sum * rescale + jnp.sum(exp_terms, -1)
    run_acc = run_acc * rescale[..., None] + jnp.einsum(
        "mqhk,khe->mqhe",
        exp_terms.astype(jnp.bfloat16),
        value_view,
        preferred_element_type=jnp.float32,
    )
    return (new_max, run_sum, run_acc)


def fresh_state(length, heads, head_size):
    return (
        jnp.full((2, length, heads), -1e30, jnp.float32),
        jnp.zeros((2, length, heads), jnp.float32),
        jnp.zeros((2, length, heads, 2 * head_size), jnp.float32),
    )


def finish(current, weights_two, gain_vec):
    run_max, run_sum, run_acc = current
    mixture = (
        run_acc[0] / run_sum[0][..., None]
        - weights_two[None, :, None] * run_acc[1] / run_sum[1][..., None]
    )
    normed = rms_norm(mixture, gain_vec)
    return normed.reshape(normed.shape[0], -1).astype(jnp.bfloat16)


def slot_numbers(flat_ids, experts):
    onehot = (flat_ids[:, None] == jnp.arange(experts, dtype=jnp.int32)[None, :]).astype(jnp.int32)
    before = jnp.cumsum(onehot, 0) - onehot
    return jnp.sum(before * onehot, 1)


def send_matrix(route_rows, experts, capacity):
    groups, sub_rows, top_count = route_rows.shape
    slot_ids = jax.vmap(lambda flat_ids: slot_numbers(flat_ids, experts))(
        route_rows.reshape(groups, -1)
    )
    group_ids = jnp.arange(groups, dtype=jnp.int32)[:, None]
    row_ids = (
        route_rows.reshape(groups, -1) * (groups * capacity) + group_ids * capacity + slot_ids
    ).reshape(-1)
    col_ids = jnp.broadcast_to(
        group_ids[:, :, None] * sub_rows + jnp.arange(sub_rows, dtype=jnp.int32)[None, :, None],
        route_rows.shape,
    ).reshape(-1)
    row_hot = (
        row_ids[:, None] == jnp.arange(experts * groups * capacity, dtype=jnp.int32)[None, :]
    ).astype(jnp.bfloat16)
    col_hot = (col_ids[:, None] == jnp.arange(groups * sub_rows, dtype=jnp.int32)[None, :]).astype(
        jnp.bfloat16
    )
    return jnp.einsum("ar,ac->rc", row_hot, col_hot, preferred_element_type=jnp.float32).astype(
        jnp.bfloat16
    )


def back_matrix(route_rows, route_weights, experts, capacity):
    sub_rows, top_count = route_rows.shape
    slot_ids = slot_numbers(route_rows.reshape(-1), experts)
    row_ids = route_rows.reshape(-1) * capacity + slot_ids
    col_ids = jnp.repeat(jnp.arange(sub_rows, dtype=jnp.int32), top_count)
    row_hot = (row_ids[:, None] == jnp.arange(experts * capacity, dtype=jnp.int32)[None, :]).astype(
        jnp.float32
    )
    tok_weighted = (col_ids[:, None] == jnp.arange(sub_rows, dtype=jnp.int32)[None, :]).astype(
        jnp.float32
    ) * route_weights.reshape(-1)[:, None]
    return jnp.einsum("at,ar->tr", tok_weighted, row_hot, precision=lax.Precision.HIGHEST)


def per_device(
    queries_a,
    keys_a,
    values_a,
    queries_b,
    keys_b,
    values_b,
    lambdas,
    head_gain_a,
    head_gain_b,
    out_a,
    out_b,
    residual,
    gain_mix,
    gain_pre,
    gain_post,
    routes,
    route_weights,
    expert_gate,
    expert_up,
    expert_down,
):
    length = queries_a.shape[0]
    heads_a = queries_a.shape[2] // DA
    heads_b = queries_b.shape[2] // DB
    head_slot = lax.axis_index("tp")
    seq_slot = lax.axis_index("sp")
    lambda_a = lax.dynamic_slice_in_dim(lambdas, head_slot * heads_a, heads_a)
    lambda_b = lax.dynamic_slice_in_dim(lambdas, HA + head_slot * heads_b, heads_b)
    groups = [
        (
            queries_a.reshape(length, 2, heads_a, DA),
            queries_b.reshape(length, 2, heads_b, DB),
            seq_slot * length + jnp.arange(length, dtype=jnp.int32),
            seq_slot * length + length - 1,
        )
    ]
    initial = tuple(
        (
            (
                fresh_state(group[2].shape[0], heads_a, DA),
                fresh_state(group[2].shape[0], heads_b, DB),
            )
            for group in groups
        )
    )
    pieces = (
        lax.all_gather(keys_a, "sp", axis=0, tiled=True),
        lax.all_gather(values_a, "sp", axis=0, tiled=True),
        lax.all_gather(keys_b, "sp", axis=0, tiled=True),
        lax.all_gather(values_b, "sp", axis=0, tiled=True),
    )
    key_count = pieces[0].shape[0]
    span_rows = 1024

    def one_span(span_index, carried):
        offset = span_index * span_rows
        parts = tuple(
            (lax.dynamic_slice_in_dim(piece_part, offset, span_rows, 0) for piece_part in pieces)
        )
        group_qa, group_qb, group_pos, group_last = groups[0]

        def compute(inner, group_qa=group_qa, group_qb=group_qb, group_pos=group_pos):
            return (
                attend(inner[0], group_qa, parts[0], parts[1], offset, group_pos, DA),
                attend(inner[1], group_qb, parts[2], parts[3], offset, group_pos, DB),
            )

        updated = [lax.cond(offset <= group_last, compute, lambda inner: inner, carried[0])]
        return tuple(updated)

    final_state = lax.fori_loop(0, key_count // span_rows, one_span, initial)
    heads_out_a = finish(final_state[0][0], lambda_a, head_gain_a)
    heads_out_b = finish(final_state[0][1], lambda_b, head_gain_b)
    mixed_rows = lax.psum_scatter(
        (
            jnp.dot(heads_out_a, out_a, preferred_element_type=jnp.float32)
            + jnp.dot(heads_out_b, out_b, preferred_element_type=jnp.float32)
        ).astype(jnp.bfloat16),
        "tp",
        scatter_dimension=0,
        tiled=True,
    ).astype(jnp.float32)
    after_mix = (residual.astype(jnp.float32) + rms_norm(mixed_rows, gain_mix)).astype(jnp.bfloat16)
    normed = rms_norm(after_mix.astype(jnp.float32), gain_pre).astype(jnp.bfloat16)
    experts = lax.axis_size("sp")
    sub_rows = residual.shape[0]
    top_count = routes.shape[1]
    capacity = min(sub_rows, (5 * sub_rows * top_count + 4 * experts - 1) // (4 * experts))
    width = residual.shape[1]
    outgoing = jnp.dot(
        send_matrix(routes[None], experts, capacity), normed, preferred_element_type=jnp.float32
    ).astype(jnp.bfloat16)
    outgoing = outgoing.reshape(experts, capacity, width)
    arrived = lax.all_to_all(outgoing, "sp", split_axis=0, concat_axis=0, tiled=True)
    sources, slot_count, columns = arrived.shape
    piece_rows = lax.all_gather(arrived.reshape(-1, columns), "tp", axis=0, tiled=True)
    gate_pre = jnp.dot(piece_rows, expert_gate[0], preferred_element_type=jnp.float32)
    up_pre = jnp.dot(piece_rows, expert_up[0], preferred_element_type=jnp.float32)
    glu_part = jnp.minimum(gate_pre, 7.0)
    lin_part = jnp.clip(up_pre, -7.0, 7.0)
    hidden = (glu_part * jax.nn.sigmoid(1.702 * glu_part) * (lin_part + 1.0)).astype(jnp.bfloat16)
    partials = jnp.dot(hidden, expert_down[0], preferred_element_type=jnp.float32)
    mine = lax.psum_scatter(partials.astype(jnp.bfloat16), "tp", scatter_dimension=0, tiled=True)
    results = mine.reshape(sources, slot_count, columns)
    returned = lax.all_to_all(results, "sp", split_axis=0, concat_axis=0, tiled=True)
    combine = back_matrix(routes, route_weights, experts, capacity)
    routed = jnp.dot(
        combine,
        returned.reshape(-1, width).astype(jnp.float32),
        precision=lax.Precision.HIGHEST,
        preferred_element_type=jnp.float32,
    )
    return (after_mix.astype(jnp.float32) + rms_norm(routed, gain_post)).astype(jnp.bfloat16)


def solution(mesh):
    in_specs = (
        P(("grp", "sp"), None, "tp"),
        P(("grp", "sp"), None, "tp"),
        P(("grp", "sp"), "tp"),
        P(("grp", "sp"), None, "tp"),
        P(("grp", "sp"), None, "tp"),
        P(("grp", "sp"), "tp"),
        P(),
        P(),
        P(),
        P("tp", None),
        P("tp", None),
        P(("grp", "sp", "tp"), None),
        P(),
        P(),
        P(),
        P(("grp", "sp", "tp"), None),
        P(("grp", "sp", "tp"), None),
        P("sp", None, "tp"),
        P("sp", None, "tp"),
        P("sp", "tp", None),
    )
    out_specs = P(("grp", "sp", "tp"), None)
    return jax.shard_map(
        per_device, mesh=mesh, in_specs=in_specs, out_specs=out_specs, check_vma=False
    )
```

profile of v0, /device:TPU:0, one launch (start us, length us, event | category | flops | bytes accessed | tf_op | source)
XLA Modules:
  0.0 503.5 jit_solution(3561112254705816321)
XLA Ops:
  6.6 2.0 copy.36
  8.6 1.8 copy.38
  10.5 1.8 copy.39
  12.4 1.8 copy.41
  14.3 1.1 copy.37
  15.4 0.8 copy.42
  16.3 0.9 copy.40
  17.1 0.1 dynamic_slice.58
  17.3 0.1 dynamic_slice.59
  17.5 24.9 %all-gather.6.cloned.1.call-done = bf16[2048,2,256]{0,2,1:T(8,128)(2,1)} async-done(((bf16[256,2,256]{0,2,1:T(8,128)(2,1)}), bf16[2048,2,256]{0,2,1:T(8,128)(2,1)}) %all-gather.6.cloned.1.call-update) | async-done | bytes 2097168 | tf_op jit(solution)/shard_map/all_gather | solution.py:149
  42.4 31.3 %all-gather.8.cloned.1.call-done = bf16[2048,512]{0,1:T(8,128)(2,1)} async-done(((bf16[256,512]{0,1:T(8,128)(2,1)}), bf16[2048,512]{0,1:T(8,128)(2,1)}) %all-gather.8.cloned.1.call-update) | async-done | bytes 2097168 | tf_op jit(solution)/shard_map/all_gather | solution.py:150
  73.7 31.3 %all-gather.10.cloned.1.call-done = bf16[2048,2,256]{0,2,1:T(8,128)(2,1)} async-done(((bf16[256,2,256]{0,2,1:T(8,128)(2,1)}), bf16[2048,2,256]{0,2,1:T(8,128)(2,1)}) %all-gather.10.cloned.1.call-update) | async-done | bytes 2097168 | tf_op jit(solution)/shard_map/all_gather | solution.py:151
  104.9 31.1 %all-gather.12.cloned.1.call-done = bf16[2048,512]{0,1:T(8,128)(2,1)} async-done(((bf16[256,512]{0,1:T(8,128)(2,1)}), bf16[2048,512]{0,1:T(8,128)(2,1)}) %all-gather.12.cloned.1.call-update) | async-done | bytes 2097168 | tf_op jit(solution)/shard_map/all_gather | solution.py:152
  136.0 0.1 broadcast_in_dim.113
  136.1 1.1 broadcast_in_dim.116
  137.3 13.8 %while.24 = (s32[]{:T(128)}, f32[2,256,2]{1,2,0:T(2,128)S(1)}, f32[2,256,2]{1,2,0:T(2,128)S(1)}, f32[2,256,2,256]{3,1,0,2:T(8,128)S(1)}, f32[2,256,4]{1,2,0:T(4,...) while((s32[]{:T(128)}, f32[2,256,2]{1,2,0:T(2,128)S(1)}, ...), condition=%wide.region_7.8_spmd.clone, body=%wide.region_0.7_spmd.clone.sunk | while | flops 1640242432 | bytes 83845752 | solution.py:173
  137.3 13.8 %conditional.3 = ((f32[2,256,2]{1,2,0:T(2,128)S(1)}, f32[2,256,2]{1,2,0:T(2,128)S(1)}, f32[2,256,2,256]{3,1,0,2:T(8,128)S(1)}, f32[2,256,4]{1,2,0:T(4,128)S(1)},...) conditional(s32[]{:T(128)} %convert_element_type.151, (f32[2,256,2]{1,2,0:T(2,128)S(1)}, ...), branch_computations={%region_1.0_spmd, %region_2.6_spmd} | conditional | flops 1640242432 | bytes 83844368 | solution.py:170
  137.3 0.2 broadcast_compare_fusion
  137.5 1.8 constant_dynamic-slice_fusion.1
  139.3 1.0 fusion.7
  140.3 1.2 fusion.8
  141.5 0.3 copy-done.1
  141.9 0.6 copy-done.2
  142.5 0.2 constant_dynamic-slice_fusion
  142.7 1.3 fusion.15
  144.1 1.5 fusion.2
  145.6 2.3 fusion.3
  148.0 2.0 fusion.21
  150.0 1.0 copy-done.6
  151.1 1.3 copy.43
  152.4 2.3 fusion.84
  154.7 1.4 fusion.65
  156.0 1.6 copy.45
  157.7 0.2 fusion.64
  157.9 1.5 fusion.57
  159.4 0.7 fusion.85
  160.2 0.2 fusion.51
  160.4 1.7 fusion.34
  162.2 0.1 copy.48
  162.3 0.1 reshape.307
  162.4 0.1 eq.111
  162.6 1.3 reduce-window.16
  163.9 0.2 slice_reduce_fusion
  164.1 1.1 reduce-window.14
  165.3 0.2 slice_reduce_fusion.1
  165.6 0.1 eq.104
  165.7 0.1 fusion.73
  165.8 0.1 fusion.75
  165.9 29.2 %reduce-scatter.3.cloned.1.call-done = bf16[128,2048]{1,0:T(8,128)(2,1)} async-done(((bf16[256,2048]{1,0:T(8,128)(2,1)}), bf16[128,2048]{1,0:T(8,128)(2,1)}) %reduce-scatter.3.cloned.1.call-update) | async-done | bytes 524304 | tf_op jit(solution)/shard_map/reduce_scatter | solution.py:176
  195.1 1.2 fusion.38
  196.4 1.5 fusion.42
  197.8 3.0 convolution_convert_fusion.1
  200.8 65.0 %all_to_all.10 = bf16[8,80,2048]{2,1,0:T(8,128)(2,1)} all-to-all(bf16[8,80,2048]{2,1,0:T(8,128)(2,1)} %bitcast.199), channel_id=1, replica_groups=mesh['grp'=2,'sp'=8,'tp'=2] {'sp'}, dimensions={0} | all-to-all | bytes 5242880 | tf_op jit(solution)/shard_map/all_to_all | solution.py:196
  265.9 66.6 %all-gather.14.cloned.1.call-done = bf16[1280,2048]{1,0:T(8,128)(2,1)} async-done(((bf16[640,2048]{1,0:T(8,128)(2,1)}), bf16[1280,2048]{1,0:T(8,128)(2,1)}) %all-gather.14.cloned.1.call-update) | async-done | bytes 5242896 | tf_op jit(solution)/shard_map/all_gather | solution.py:198
  332.5 10.2 %fusion.26 = f32[1280,1024]{1,0:T(8,128)} fusion(bf16[1280,2048]{1,0:T(8,128)(2,1)} %all-gather.14.cloned.1.call-done, bf16[1,2048,1024]{2,1,0:T(8,128)(2,1)} %param.41), kind=kOutput, calls=%fused_computation.34 | convolution fusion | flops 5368709120 | bytes 14680064 | tf_op jit(solution)/shard_map/dot_general | solution.py:199
  342.7 18.7 %convolution_convert_fusion = bf16[1280,2048]{1,0:T(8,128)(2,1)} fusion(bf16[1,1024,2048]{2,1,0:T(8,128)(2,1)} %param.43, f32[1280,1024]{1,0:T(8,128)} %fusion.26, bf16[1280,2048]{1,0:T(8,128)(2,1)} %all-gather.14.cloned.1.call-done, bf16[1,2048,1024]{2,1,0:T(8,128)(2,1)} %param.42), kind=kOutput, calls=%fused_computation.30 | convolution fusion | flops 10753146880 | bytes 24117248 | tf_op jit(solution)/shard_map/dot_general | solution.py:204
  361.4 65.9 %reduce-scatter.5.cloned.1.call-done = bf16[640,2048]{1,0:T(8,128)(2,1)} async-done(((bf16[1280,2048]{1,0:T(8,128)(2,1)}), bf16[640,2048]{1,0:T(8,128)(2,1)}) %reduce-scatter.5.cloned.1.call-update) | async-done | bytes 2621456 | tf_op jit(solution)/shard_map/reduce_scatter | solution.py:205
  427.3 4.7 all-to-all-start.1
  432.1 0.1 copy.47
  432.2 0.1 mul.301
  432.3 0.8 fusion.35
  433.1 59.3 %all-to-all-done.1 = bf16[8,80,2048]{2,1,0:T(8,128)(2,1)} async-done(((bf16[8,80,2048]{2,1,0:T(8,128)(2,1)}), bf16[8,80,2048]{2,1,0:T(8,128)(2,1)}, u32[]{:S(2)}, u32[]{:S(2)}) %all-to-all-start.1) | async-done | bytes 2621472 | tf_op jit(solution)/shard_map/all_to_all | solution.py:207
  492.4 3.2 multiply_reduce_fusion
  495.7 1.0 fusion.45
  (85 shorter events, 0.9 us)
Async XLA Ops:
  6.5 152.9 %copy-start = (bf16[512,2048]{1,0:T(8,128)(2,1)S(1)}, bf16[512,2048]{1,0:T(8,128)(2,1)}, u32[]{:S(2)}) copy-start(bf16[512,2048]{1,0:T(8,128)(2,1)} %param.33) | copy-start | bytes 6291460
  6.5 9.7 %copy-start.9 = (bf16[256,2,256]{2,1,0:T(2,128)(2,1)S(1)}, bf16[256,2,256]{2,1,0:T(2,128)(2,1)}, u32[]{:S(2)}) copy-start(bf16[256,2,256]{2,1,0:T(2,128)(2,1)} %param.27) | copy-start | bytes 786436
  6.5 10.6 %copy-start.15 = (f32[256]{0:T(256)S(1)}, f32[256]{0:T(256)}, u32[]{:S(2)}) copy-start(f32[256]{0:T(256)} %param.31) | copy-start | bytes 3076
  6.5 10.6 %copy-start.17 = (f32[12]{0:T(128)S(1)}, f32[12]{0:T(128)}, u32[]{:S(2)}) copy-start(f32[12]{0:T(128)} %param.30) | copy-start | bytes 148
  6.5 10.8 %copy-start.16 = (f32[128]{0:T(128)S(1)}, f32[128]{0:T(128)}, u32[]{:S(2)}) copy-start(f32[128]{0:T(128)} %param.32) | copy-start | bytes 1540
  6.5 35.8 %all-gather.6.cloned.1.call-start = ((), (), s32[]{:S(2)}) async-start(), calls=%async_computation.4 | async-start | bytes 2359296 | tf_op jit(solution)/shard_map/all_gather | solution.py:149
  8.6 65.1 %all-gather.8.cloned.1.call-start = ((), (), s32[]{:S(2)}) async-start(), calls=%async_computation.5 | async-start | bytes 2359296 | tf_op jit(solution)/shard_map/all_gather | solution.py:150
  10.5 94.5 %all-gather.10.cloned.1.call-start = ((), (), s32[]{:S(2)}) async-start(), calls=%async_computation.6 | async-start | bytes 2359296 | tf_op jit(solution)/shard_map/all_gather | solution.py:151
  12.4 123.7 %all-gather.12.cloned.1.call-start = ((), (), s32[]{:S(2)}) async-start(), calls=%async_computation.7 | async-start | bytes 2359296 | tf_op jit(solution)/shard_map/all_gather | solution.py:152
  14.3 180.8 %reduce-scatter.3.cloned.1.call-start = ((), (), s32[]{:S(2)}) async-start(), calls=%async_computation.8 | async-start | bytes 1572864 | tf_op jit(solution)/shard_map/reduce_scatter | solution.py:176
  137.5 1.8 copy-start.3
  140.3 1.6 copy-start.1
  140.3 2.2 copy-start.2
  142.5 1.6 copy-start.4
  145.6 2.4 copy-start.5
  150.0 1.0 copy-start.6
  157.7 2.7 copy-start.7
  160.2 2.0 copy-start.13
  160.2 36.2 %copy-start.8 = (bf16[128,2048]{1,0:T(8,128)(2,1)S(1)}, bf16[128,2048]{1,0:T(8,128)(2,1)}, u32[]{:S(2)}) copy-start(bf16[128,2048]{1,0:T(8,128)(2,1)} %param.35) | copy-start | bytes 1572868
  160.2 36.2 %copy-start.10 = (f32[2048]{0:T(1024)S(1)}, f32[2048]{0:T(1024)}, u32[]{:S(2)}) copy-start(f32[2048]{0:T(1024)} %param.36) | copy-start | bytes 24580
  160.4 37.4 %copy-start.11 = (f32[2048]{0:T(1024)S(1)}, f32[2048]{0:T(1024)}, u32[]{:S(2)}) copy-start(f32[2048]{0:T(1024)} %param.37) | copy-start | bytes 24580
  162.2 170.3 %all-gather.14.cloned.1.call-start = ((), (), s32[]{:S(2)}) async-start(), calls=%async_computation.9 | async-start | bytes 7864320 | tf_op jit(solution)/shard_map/all_gather | solution.py:198
  265.8 161.5 %reduce-scatter.5.cloned.1.call-start = ((), (), s32[]{:S(2)}) async-start(), calls=%async_computation.10 | async-start | bytes 7864320 | tf_op jit(solution)/shard_map/reduce_scatter | solution.py:205
  361.4 70.7 %copy-start.14 = (f32[128,4]{0,1:T(4,128)S(1)}, f32[128,4]{0,1:T(4,128)}, u32[]{:S(2)}) copy-start(f32[128,4]{0,1:T(4,128)} %param.40) | copy-start | bytes 6148
  427.3 68.3 %copy-start.12 = (f32[2048]{0:T(1024)S(1)}, f32[2048]{0:T(1024)}, u32[]{:S(2)}) copy-start(f32[2048]{0:T(1024)} %param.38) | copy-start | bytes 24580
  427.3 65.1 %all-to-all-start.1 = ((bf16[8,80,2048]{2,1,0:T(8,128)(2,1)}), bf16[8,80,2048]{2,1,0:T(8,128)(2,1)}, u32[]{:S(2)}, u32[]{:S(2)}) async-start(bf16[8,80,2048]{2,1,0:T(8,128)(2,1)} %bitcast.202), calls=%async_computation.3 | async-start | bytes 5242880 | tf_op jit(solution)/shard_map/all_to_all | solution.py:207
Sparse Core Ops, SparseCore 0:
  8.9 33.3 all-gather.5
  44.0 29.6 all-gather.7
  75.3 29.6 all-gather.9
  106.4 29.6 all-gather.11
  162.3 32.7 reduce-scatter.2
  266.0 66.4 all-gather.13
  361.5 65.7 reduce-scatter.4
where the time goes:
time: 504 us
  waiting for transfers between devices  340 us (67%)
  blocking collectives  65 us (13%)
  matrix products  44.2 us (9%)
  local copies, waits for them, and re-layouts  22.1 us (4%)
  between operations  13.8 us (3%)
  other arithmetic  13.5 us (3%)
  starting transfers between devices  5.04 us (1%)
    all_gather x1, waiting for transfers between devices, per_device(): lax.all_gather(arrived.reshape(-1, columns), 'tp', axis=0, tiled=True)  66.6 us
    reduce_scatter x1, waiting for transfers between devices, per_device(): lax.psum_scatter(partials.astype(jnp.bfloat16), 'tp', scatter_dimension=0...  65.9 us
    all_to_all x1, blocking collectives, per_device(): lax.all_to_all(outgoing, 'sp', split_axis=0, concat_axis=0, tiled=True)  65 us
    all_to_all x1, waiting for transfers between devices, per_device(): lax.all_to_all(results, 'sp', split_axis=0, concat_axis=0, tiled=True)  59.3 us
    all_gather x1, waiting for transfers between devices, per_device(): lax.all_gather(values_a, 'sp', axis=0, tiled=True)  31.3 us
    all_gather x1, waiting for transfers between devices, per_device(): lax.all_gather(keys_b, 'sp', axis=0, tiled=True)  31.3 us
    all_gather x1, waiting for transfers between devices, per_device(): lax.all_gather(values_b, 'sp', axis=0, tiled=True)  31.1 us
    reduce_scatter x1, waiting for transfers between devices, per_device(): lax.psum_scatter((jnp.dot(heads_out_a, out_a, preferred_element_type=jnp....  29.2 us
  transfers between devices with their start and end apart: 8, of which 8 were waited for; matrix products, arithmetic and copies ran while one was open for 3% of the time, Pallas kernels for 0%

commit v1 on v0

--- a/solution.py
+++ b/solution.py
@@ -6,6 +6,27 @@
 HA = 4
 DA = 128
 DB = 64
+
+
+def collect(shard, axis, dim):
+    size, index, span = (lax.axis_size(axis), lax.axis_index(axis), shard.shape[dim])
+    upward = [(i, (i + 1) % size) for i in range(size)]
+    left = [(i, (i - 1) % size) for i in range(size)]
+    result = jnp.zeros((*shard.shape[:dim], size * span, *shard.shape[dim + 1 :]), shard.dtype)
+    result = lax.dynamic_update_slice_in_dim(result, shard, index * span, axis=dim)
+    from_left = from_right = shard
+    half = size // 2
+    for turn in range(1, half + 1):
+        from_left = lax.ppermute(from_left, axis, upward)
+        result = lax.dynamic_update_slice_in_dim(
+            result, from_left, (index - turn) % size * span, axis=dim
+        )
+        if turn < size - half:
+            from_right = lax.ppermute(from_right, axis, left)
+            result = lax.dynamic_update_slice_in_dim(
+                result, from_right, (index + turn) % size * span, axis=dim
+            )
+    return result
 
 
 def rms_norm(values, gain_vec):
@@ -149,7 +170,7 @@
         lax.all_gather(keys_a, "sp", axis=0, tiled=True),
         lax.all_gather(values_a, "sp", axis=0, tiled=True),
         lax.all_gather(keys_b, "sp", axis=0, tiled=True),
-        lax.all_gather(values_b, "sp", axis=0, tiled=True),
+        collect(values_b, "sp", 0),
     )
     key_count = pieces[0].shape[0]
     span_rows = 1024

time: 504 us -> 485 us (0.962)
  waiting for transfers between devices: 340 us -> 291 us
  starting transfers between devices: 5.04 us -> 23.7 us
  local copies, waits for them, and re-layouts: 22.1 us -> 33.2 us
    all_gather x1 -> x0, waiting for transfers between devices: 31.1 us -> none  [per_device(): lax.all_gather(values_b, 'sp', axis=0, tiled=True)]
    all_gather x1, waiting for transfers between devices: 24.9 us -> 0.01 us  [per_device(): lax.all_gather(keys_a, 'sp', axis=0, tiled=True)]
    ppermute x0 -> x7, starting transfers between devices: none -> 18.5 us  [the longest x3 10.9 us: collect(): from_right = lax.ppermute(from_right, axis, left)]
    ppermute x0 -> x7, waiting for transfers between devices: none -> 11.2 us  [the longest x3 6.5 us: collect(): from_right = lax.ppermute(from_right, axis, left)]
    dynamic_update_slice x0 -> x8, local copies, waits for them, and re-layouts: none -> 6.02 us  [the longest x4 3.01 us: collect(): lax.dynamic_update_slice_in_dim(result, from_left, (index - turn) % size...]
    unnamed x37 -> x29, local copies, waits for them, and re-layouts: 10.6 us -> 11.4 us
  transfers between devices with their start and end apart: 8 -> 14, of which waited for: 8 -> 10; matrix products, arithmetic and copies ran while one was open for 3% -> 5% of each run, Pallas kernels for 0% -> 0%
where the time goes in v1:
time: 485 us
  waiting for transfers between devices  291 us (60%)
  blocking collectives  65 us (13%)
  matrix products  44.2 us (9%)
  local copies, waits for them, and re-layouts  33.2 us (7%)
  starting transfers between devices  23.7 us (5%)
  between operations  13.7 us (3%)
  other arithmetic  13.3 us (3%)
    all_gather x1, waiting for transfers between devices, per_device(): lax.all_gather(arrived.reshape(-1, columns), 'tp', axis=0, tiled=True)  66.6 us
    reduce_scatter x1, waiting for transfers between devices, per_device(): lax.psum_scatter(partials.astype(jnp.bfloat16), 'tp', scatter_dimension=0...  65.9 us
    all_to_all x1, blocking collectives, per_device(): lax.all_to_all(outgoing, 'sp', split_axis=0, concat_axis=0, tiled=True)  65 us
    all_to_all x1, waiting for transfers between devices, per_device(): lax.all_to_all(results, 'sp', split_axis=0, concat_axis=0, tiled=True)  59.3 us
    all_gather x1, waiting for transfers between devices, per_device(): lax.all_gather(keys_b, 'sp', axis=0, tiled=True)  31.3 us
    reduce_scatter x1, waiting for transfers between devices, per_device(): lax.psum_scatter((jnp.dot(heads_out_a, out_a, preferred_element_type=jnp....  29.8 us
    all_gather x1, waiting for transfers between devices, per_device(): lax.all_gather(values_a, 'sp', axis=0, tiled=True)  27.1 us
    dot_general x1, matrix products, per_device(): jnp.dot(hidden, expert_down[0], preferred_element_type=jnp.float32)  18.7 us
  transfers between devices with their start and end apart: 14, of which 10 were waited for; matrix products, arithmetic and copies ran while one was open for 5% of the time, Pallas kernels for 0%

profile of v1, /device:TPU:0, one launch (start us, length us, event | category | flops | bytes accessed | tf_op | source)
XLA Modules:
  0.0 484.5 jit_solution(8779997499716233622)
XLA Ops:
  6.5 2.0 copy.36
  8.6 1.8 copy.38
  10.5 1.8 copy.39
  12.3 1.1 copy.41
  14.0 4.1 collective-permute-start.1
  18.1 0.7 dynamic_slice.59
  20.2 0.7 dynamic_slice.58
  20.9 1.3 collective-permute-done
  22.3 6.5 %collective-permute-done.1 = bf16[256,512]{0,1:T(8,128)(2,1)S(1)} collective-permute-done((bf16[256,512]{0,1:T(8,128)(2,1)S(1)}, bf16[256,512]{0,1:T(8,128)(2,1)S(1)}, u32[]{:S(2)}, u32[]{:S(2)}) %collective-permute-start.1) | collective-permute-done | bytes 262176 | tf_op jit(solution)/shard_map/ppermute | solution.py:25
  28.8 3.7 collective-permute-start.3
  32.6 1.6 broadcast_in_dim.120
  34.2 0.8 constant_dynamic-update-slice_fusion.7
  34.9 1.1 copy.37
  36.0 0.8 copy.44
  36.9 1.8 copy.40
  38.7 2.6 collective-permute-start.4
  41.3 0.8 constant_dynamic-update-slice_fusion.6
  42.0 0.7 constant_dynamic-update-slice_fusion.5
  42.8 3.1 collective-permute-start.5
  45.9 0.7 constant_dynamic-update-slice_fusion.4
  46.7 0.9 collective-permute-done.4
  47.5 4.4 collective-permute-start.6
  51.9 0.7 constant_dynamic-update-slice_fusion.3
  52.7 0.7 constant_dynamic-update-slice_fusion.2
  53.4 0.8 constant_dynamic-update-slice_fusion.1
  54.1 2.5 collective-permute-done.6
  56.6 0.8 constant_dynamic-update-slice_fusion
  57.4 27.1 %all-gather.7.cloned.1.call-done = bf16[2048,512]{0,1:T(8,128)(2,1)} async-done(((bf16[256,512]{0,1:T(8,128)(2,1)}), bf16[2048,512]{0,1:T(8,128)(2,1)}) %all-gather.7.cloned.1.call-update) | async-done | bytes 2097168 | tf_op jit(solution)/shard_map/all_gather | solution.py:171
  84.5 31.3 %all-gather.9.cloned.1.call-done = bf16[2048,2,256]{0,2,1:T(8,128)(2,1)} async-done(((bf16[256,2,256]{0,2,1:T(8,128)(2,1)}), bf16[2048,2,256]{0,2,1:T(8,128)(2,1)}) %all-gather.9.cloned.1.call-update) | async-done | bytes 2097168 | tf_op jit(solution)/shard_map/all_gather | solution.py:172
  115.9 1.1 broadcast_in_dim.119
  117.0 14.4 %while.24 = (s32[]{:T(128)}, f32[2,256,2]{1,2,0:T(2,128)S(1)}, f32[2,256,2]{1,2,0:T(2,128)S(1)}, f32[2,256,2,256]{3,1,0,2:T(8,128)S(1)}, f32[2,256,4]{1,2,0:T(4,...) while((s32[]{:T(128)}, f32[2,256,2]{1,2,0:T(2,128)S(1)}, ...), condition=%wide.region_7.8_spmd.clone, body=%wide.region_0.7_spmd.clone.sunk | while | flops 1640242432 | bytes 75457112 | solution.py:194
  117.0 14.4 %conditional.3 = ((f32[2,256,2]{1,2,0:T(2,128)S(1)}, f32[2,256,2]{1,2,0:T(2,128)S(1)}, f32[2,256,2,256]{3,1,0,2:T(8,128)S(1)}, f32[2,256,4]{1,2,0:T(4,128)S(1)},...) conditional(s32[]{:T(128)} %convert_element_type.151, (f32[2,256,2]{1,2,0:T(2,128)S(1)}, ...), branch_computations={%region_1.1_spmd, %region_2.6_spmd} | conditional | flops 1640242432 | bytes 75455728 | solution.py:191
  117.3 1.8 constant_dynamic-slice_fusion.1
  119.0 1.0 fusion.7
  120.0 1.2 fusion.8
  121.6 1.4 constant_dynamic-slice_fusion
  123.1 1.3 fusion.15
  124.4 1.5 fusion.2
  126.0 2.3 fusion.3
  128.4 2.0 fusion.21
  130.4 1.0 copy-done.5
  131.4 1.3 copy.45
  132.7 2.3 fusion.84
  135.0 1.4 fusion.65
  136.4 1.6 copy.47
  138.3 1.5 fusion.57
  139.8 0.7 fusion.85
  140.8 1.7 fusion.34
  143.1 1.1 reduce-window.16
  144.5 1.1 reduce-window.14
  146.3 29.8 %reduce-scatter.3.cloned.1.call-done = bf16[128,2048]{1,0:T(8,128)(2,1)} async-done(((bf16[256,2048]{1,0:T(8,128)(2,1)}), bf16[128,2048]{1,0:T(8,128)(2,1)}) %reduce-scatter.3.cloned.1.call-update) | async-done | bytes 524304 | tf_op jit(solution)/shard_map/reduce_scatter | solution.py:197
  176.1 1.2 fusion.38
  177.3 1.5 fusion.42
  178.8 3.0 convolution_convert_fusion.1
  181.8 65.0 %all_to_all.10 = bf16[8,80,2048]{2,1,0:T(8,128)(2,1)} all-to-all(bf16[8,80,2048]{2,1,0:T(8,128)(2,1)} %bitcast.199), channel_id=1, replica_groups=mesh['grp'=2,'sp'=8,'tp'=2] {'sp'}, dimensions={0} | all-to-all | bytes 5242880 | tf_op jit(solution)/shard_map/all_to_all | solution.py:217
  246.9 66.6 %all-gather.11.cloned.1.call-done = bf16[1280,2048]{1,0:T(8,128)(2,1)} async-done(((bf16[640,2048]{1,0:T(8,128)(2,1)}), bf16[1280,2048]{1,0:T(8,128)(2,1)}) %all-gather.11.cloned.1.call-update) | async-done | bytes 5242896 | tf_op jit(solution)/shard_map/all_gather | solution.py:219
  313.5 10.2 %fusion.26 = f32[1280,1024]{1,0:T(8,128)} fusion(bf16[1280,2048]{1,0:T(8,128)(2,1)} %all-gather.11.cloned.1.call-done, bf16[1,2048,1024]{2,1,0:T(8,128)(2,1)} %param.41), kind=kOutput, calls=%fused_computation.34 | convolution fusion | flops 5368709120 | bytes 14680064 | tf_op jit(solution)/shard_map/dot_general | solution.py:220
  323.7 18.7 %convolution_convert_fusion = bf16[1280,2048]{1,0:T(8,128)(2,1)} fusion(bf16[1,1024,2048]{2,1,0:T(8,128)(2,1)} %param.43, f32[1280,1024]{1,0:T(8,128)} %fusion.26, bf16[1280,2048]{1,0:T(8,128)(2,1)} %all-gather.11.cloned.1.call-done, bf16[1,2048,1024]{2,1,0:T(8,128)(2,1)} %param.42), kind=kOutput, calls=%fused_computation.30 | convolution fusion | flops 10753146880 | bytes 24117248 | tf_op jit(solution)/shard_map/dot_general | solution.py:225
  342.4 65.9 %reduce-scatter.5.cloned.1.call-done = bf16[640,2048]{1,0:T(8,128)(2,1)} async-done(((bf16[1280,2048]{1,0:T(8,128)(2,1)}), bf16[640,2048]{1,0:T(8,128)(2,1)}) %reduce-scatter.5.cloned.1.call-update) | async-done | bytes 2621456 | tf_op jit(solution)/shard_map/reduce_scatter | solution.py:226
  408.3 4.8 all-to-all-start.1
  413.4 0.8 fusion.35
  414.1 59.3 %all-to-all-done.1 = bf16[8,80,2048]{2,1,0:T(8,128)(2,1)} async-done(((bf16[8,80,2048]{2,1,0:T(8,128)(2,1)}), bf16[8,80,2048]{2,1,0:T(8,128)(2,1)}, u32[]{:S(2)}, u32[]{:S(2)}) %all-to-all-start.1) | async-done | bytes 2621472 | tf_op jit(solution)/shard_map/all_to_all | solution.py:228
  473.4 3.2 multiply_reduce_fusion
  476.7 1.0 fusion.45
  (95 shorter events, 5.2 us)
Async XLA Ops:
  6.5 133.2 %copy-start = (bf16[512,2048]{1,0:T(8,128)(2,1)S(1)}, bf16[512,2048]{1,0:T(8,128)(2,1)}, u32[]{:S(2)}) copy-start(bf16[512,2048]{1,0:T(8,128)(2,1)} %param.33) | copy-start | bytes 6291460
  6.5 50.9 %all-gather.5.cloned.1.call-start = ((), (), s32[]{:S(2)}) async-start(), calls=%async_computation.4 | async-start | bytes 2359296 | tf_op jit(solution)/shard_map/all_gather | solution.py:170
  8.5 76.0 %all-gather.7.cloned.1.call-start = ((), (), s32[]{:S(2)}) async-start(), calls=%async_computation.5 | async-start | bytes 2359296 | tf_op jit(solution)/shard_map/all_gather | solution.py:171
  10.4 105.4 %all-gather.9.cloned.1.call-start = ((), (), s32[]{:S(2)}) async-start(), calls=%async_computation.6 | async-start | bytes 2359296 | tf_op jit(solution)/shard_map/all_gather | solution.py:172
  12.3 163.8 %reduce-scatter.3.cloned.1.call-start = ((), (), s32[]{:S(2)}) async-start(), calls=%async_computation.7 | async-start | bytes 1572864 | tf_op jit(solution)/shard_map/reduce_scatter | solution.py:197
  13.4 8.8 %collective-permute-start = (bf16[256,512]{0,1:T(8,128)(2,1)S(1)}, bf16[256,512]{0,1:T(8,128)(2,1)S(1)}, u32[]{:S(2)}, u32[]{:S(2)}) collective-permute-start(bf16[256,512]{0,1:T(8,128)(2,1)S(1)} %copy.41), channel_id=1, source_target_pairs={{0,2},{2,4},{4,6},{6,8},{8,10},{10,12},{12,14},{14,0},{1,3},{3,5},... | collective-permute-start | bytes 786440 | tf_op jit(solution)/shard_map/ppermute | solution.py:20
  14.0 14.9 %collective-permute-start.1 = (bf16[256,512]{0,1:T(8,128)(2,1)S(1)}, bf16[256,512]{0,1:T(8,128)(2,1)S(1)}, u32[]{:S(2)}, u32[]{:S(2)}) collective-permute-start(bf16[256,512]{0,1:T(8,128)(2,1)S(1)} %copy.41), channel_id=1, source_target_pairs={{0,14},{2,0},{4,2},{6,4},{8,6},{10,8},{12,10},{14,12},{1,15},{3,1}... | collective-permute-start | bytes 786440 | tf_op jit(solution)/shard_map/ppermute | solution.py:25
  22.3 16.4 %collective-permute-start.2 = (bf16[256,512]{0,1:T(8,128)(2,1)S(1)}, bf16[256,512]{0,1:T(8,128)(2,1)S(1)}, u32[]{:S(2)}, u32[]{:S(2)}) collective-permute-start(bf16[256,512]{0,1:T(8,128)(2,1)S(1)} %collective-permute-done), channel_id=1, source_target_pairs={{0,2},{2,4},{4,6},{6,8},{8,10},{10,12},{12,14},{14,0},{1,3},{3,5},... | collective-permute-start | bytes 786440 | tf_op jit(solution)/shard_map/ppermute | solution.py:20
  28.8 13.9 %collective-permute-start.3 = (bf16[256,512]{0,1:T(8,128)(2,1)S(1)}, bf16[256,512]{0,1:T(8,128)(2,1)S(1)}, u32[]{:S(2)}, u32[]{:S(2)}) collective-permute-start(bf16[256,512]{0,1:T(8,128)(2,1)S(1)} %collective-permute-done.1), channel_id=1, source_target_pairs={{0,14},{2,0},{4,2},{6,4},{8,6},{10,8},{12,10},{14,12},{1,15},{3,1}... | collective-permute-start | bytes 786440 | tf_op jit(solution)/shard_map/ppermute | solution.py:25
  38.7 8.9 %collective-permute-start.4 = (bf16[256,512]{0,1:T(8,128)(2,1)S(1)}, bf16[256,512]{0,1:T(8,128)(2,1)S(1)}, u32[]{:S(2)}, u32[]{:S(2)}) collective-permute-start(bf16[256,512]{0,1:T(8,128)(2,1)S(1)} %collective-permute-done.2), channel_id=1, source_target_pairs={{0,2},{2,4},{4,6},{6,8},{8,10},{10,12},{12,14},{14,0},{1,3},{3,5},... | collective-permute-start | bytes 786440 | tf_op jit(solution)/shard_map/ppermute | solution.py:20
  42.8 10.6 %collective-permute-start.5 = (bf16[256,512]{0,1:T(8,128)(2,1)S(1)}, bf16[256,512]{0,1:T(8,128)(2,1)S(1)}, u32[]{:S(2)}, u32[]{:S(2)}) collective-permute-start(bf16[256,512]{0,1:T(8,128)(2,1)S(1)} %collective-permute-done.3), channel_id=1, source_target_pairs={{0,14},{2,0},{4,2},{6,4},{8,6},{10,8},{12,10},{14,12},{1,15},{3,1}... | collective-permute-start | bytes 786440 | tf_op jit(solution)/shard_map/ppermute | solution.py:25
  47.5 9.1 %collective-permute-start.6 = (bf16[256,512]{0,1:T(8,128)(2,1)S(1)}, bf16[256,512]{0,1:T(8,128)(2,1)S(1)}, u32[]{:S(2)}, u32[]{:S(2)}) collective-permute-start(bf16[256,512]{0,1:T(8,128)(2,1)S(1)} %collective-permute-done.4), channel_id=1, source_target_pairs={{0,2},{2,4},{4,6},{6,8},{8,10},{10,12},{12,14},{14,0},{1,3},{3,5},... | collective-permute-start | bytes 786440 | tf_op jit(solution)/shard_map/ppermute | solution.py:20
  117.3 1.8 copy-start.2
  120.0 1.6 copy-start.1
  121.6 2.8 copy-start.3
  126.0 2.4 copy-start.4
  130.4 1.1 copy-start.5
  138.0 2.7 copy-start.6
  140.5 2.3 copy-start.11
  140.5 36.8 %copy-start.7 = (bf16[128,2048]{1,0:T(8,128)(2,1)S(1)}, bf16[128,2048]{1,0:T(8,128)(2,1)}, u32[]{:S(2)}) copy-start(bf16[128,2048]{1,0:T(8,128)(2,1)} %param.35) | copy-start | bytes 1572868
  140.5 36.8 %copy-start.8 = (f32[2048]{0:T(1024)S(1)}, f32[2048]{0:T(1024)}, u32[]{:S(2)}) copy-start(f32[2048]{0:T(1024)} %param.36) | copy-start | bytes 24580
  140.8 38.0 %copy-start.9 = (f32[2048]{0:T(1024)S(1)}, f32[2048]{0:T(1024)}, u32[]{:S(2)}) copy-start(f32[2048]{0:T(1024)} %param.37) | copy-start | bytes 24580
  142.5 171.0 %all-gather.11.cloned.1.call-start = ((), (), s32[]{:S(2)}) async-start(), calls=%async_computation.8 | async-start | bytes 7864320 | tf_op jit(solution)/shard_map/all_gather | solution.py:219
  246.8 161.5 %reduce-scatter.5.cloned.1.call-start = ((), (), s32[]{:S(2)}) async-start(), calls=%async_computation.9 | async-start | bytes 7864320 | tf_op jit(solution)/shard_map/reduce_scatter | solution.py:226
  342.4 70.7 %copy-start.12 = (f32[128,4]{0,1:T(4,128)S(1)}, f32[128,4]{0,1:T(4,128)}, u32[]{:S(2)}) copy-start(f32[128,4]{0,1:T(4,128)} %param.40) | copy-start | bytes 6148
  408.3 68.3 %copy-start.10 = (f32[2048]{0:T(1024)S(1)}, f32[2048]{0:T(1024)}, u32[]{:S(2)}) copy-start(f32[2048]{0:T(1024)} %param.38) | copy-start | bytes 24580
  408.3 65.1 %all-to-all-start.1 = ((bf16[8,80,2048]{2,1,0:T(8,128)(2,1)}), bf16[8,80,2048]{2,1,0:T(8,128)(2,1)}, u32[]{:S(2)}, u32[]{:S(2)}) async-start(bf16[8,80,2048]{2,1,0:T(8,128)(2,1)} %bitcast.202), calls=%async_computation.3 | async-start | bytes 5242880 | tf_op jit(solution)/shard_map/all_to_all | solution.py:228
Sparse Core Ops, SparseCore 0:
  8.9 44.2 all-gather.4
  54.8 29.6 all-gather.6
  86.1 29.6 all-gather.8
  142.6 33.3 reduce-scatter.2
  246.9 66.5 all-gather.10
  342.5 65.7 reduce-scatter.4
